TPU v7x, 32 devices: a whole 2x2x4 slice. The times are simulated.
32 devices in a mesh: grp: 2 (over y), fs: 4 (over z), tp: 4 (over x, core).
Axes of the slice: x: 2, y: 2, z: 4, core: 2. Of those that a mesh axis runs over, the one named last changes fastest.
Arguments:
- tokens: bfloat16 [8192, 2048], P(('grp', 'fs'), 'tp'), parts along dimension 0, may hold values from -6 to 6
- norm1_gain: float32 [2048], replicated, may hold values from 0.1 to 1.9
- weight_u: float32 [2048, 1024], P('fs', 'tp'), may hold values from -0.125 to 0.125
- weight_v: float32 [2048, 1024], P('fs', 'tp'), may hold values from -0.125 to 0.125
- scale_u: float32 [1024], P('tp'), may hold values from 0.5 to 2
- scale_v: float32 [1024], P('tp'), may hold values from 0.05 to 4.5
- mix_gain: float32 [1024], P('tp'), may hold values from 0.1 to 1.9
- spatial_weight: float32 [4, 128, 128], replicated, may hold values from -0.5 to 0.5
- spatial_bias: float32 [4, 128], replicated, may hold values from 0.5 to 1.5
- weight_out: float32 [1024, 2048], P('tp', 'fs'), may hold values from -0.1875 to 0.1875
- scale_out: float32 [2048], P('fs'), may hold values from 0.5 to 2
- norm2_gain: float32 [2048], replicated, may hold values from 0.1 to 1.9
- weight_up: float32 [2048, 8192], P('fs', 'tp'), may hold values from -0.125 to 0.125
- scale_up: float32 [8192], P('tp'), may hold values from 0.5 to 2
- weight_down: float32 [8192, 2048], P('tp', 'fs'), may hold values from -0.0625 to 0.0625
- scale_down: float32 [2048], P('fs'), may hold values from 0.5 to 2
Outputs:
- result: bfloat16 [8192, 2048], P(('grp', 'fs'), 'tp'), parts along dimension 0
There are 2 independent parts, one for each index of `grp`. A program takes and returns all parts, laid end to end along the dimension named above; an argument that names none is the same for every part. Nothing has to cross between parts.
All inputs are finite; a program needn't handle non-finite values.
Results may differ from a plain program's by a relative error of at most 0.023.
Values may be sent and summed in bfloat16 or wider, within the bound.
A program may use at most 128 MiB of HBM per device.

v0:
```python
import jax
import jax.numpy as jnp
from jax import lax
from jax.sharding import PartitionSpec as P

GM_W = 1024
GROUPS = 4
BLOCK = 128


def per_device(
    tokens,
    norm1_gain,
    weight_u,
    weight_v,
    scale_u,
    scale_v,
    mix_gain,
    spatial_weight,
    spatial_bias,
    weight_out,
    scale_out,
    norm2_gain,
    weight_up,
    scale_up,
    weight_down,
    scale_down,
):
    feature_count = norm1_gain.shape[0]
    out_scales, down_scales = (
        lax.all_gather(scale_out, "fs", axis=0, tiled=True),
        lax.all_gather(scale_down, "fs", axis=0, tiled=True),
    )
    full_u, full_v = (
        lax.all_gather(weight_u.astype(jnp.bfloat16), "fs", axis=0, tiled=True),
        lax.all_gather(weight_v.astype(jnp.bfloat16), "fs", axis=0, tiled=True),
    )
    widened_in = tokens.astype(jnp.float32)
    squares_in = lax.psum(jnp.sum(widened_in * widened_in, axis=1), "tp")
    inverse_in = lax.rsqrt(squares_in / feature_count + 1e-06)[:, None]
    gain_piece = norm1_gain
    normed_piece = (
        lax.all_gather(tokens, "tp", axis=1, tiled=True).astype(jnp.float32)
        * inverse_in
        * gain_piece
    ).astype(jnp.bfloat16)
    pre_u = jnp.dot(normed_piece, full_u, preferred_element_type=jnp.float32)
    pre_v = jnp.dot(normed_piece, full_v, preferred_element_type=jnp.float32)
    gate_u = jax.nn.gelu(pre_u * scale_u)
    act_v = jax.nn.gelu(pre_v * scale_v)
    local_width = act_v.shape[1]
    row_sums, row_squares = lax.psum((jnp.sum(act_v, axis=1), jnp.sum(act_v * act_v, axis=1)), "tp")
    row_mean = (row_sums / GM_W)[:, None]
    square = (row_squares / GM_W)[:, None]
    v_norm = (
        (act_v - row_mean) * lax.rsqrt(square - row_mean * row_mean + 1e-06) * mix_gain
    ).astype(jnp.bfloat16)
    group_index = lax.axis_index("tp") * local_width // (GM_W // GROUPS)
    lower_mask = jnp.tril(jnp.ones((BLOCK, BLOCK), jnp.float32))
    spatial_mask = (
        lax.dynamic_index_in_dim(spatial_weight, group_index, 0, keepdims=False) * lower_mask
    ).astype(jnp.bfloat16)
    block_bias = lax.dynamic_index_in_dim(spatial_bias, group_index, 0, keepdims=False)
    blocks = v_norm.reshape(-1, BLOCK, local_width)
    mixed_cols = jnp.einsum("ts,nsc->ntc", spatial_mask, blocks, preferred_element_type=jnp.float32)
    mixed_cols = mixed_cols + block_bias[None, :, None]
    gated = (gate_u * mixed_cols.reshape(-1, local_width)).astype(jnp.bfloat16)
    out_rounded = weight_out.astype(jnp.bfloat16)
    full_out = lax.all_gather(out_rounded, "fs", axis=1, tiled=True)
    columns = full_out
    piece_scale = out_scales
    product = lax.dot_general(
        columns, gated, (((0,), (1,)), ((), ())), preferred_element_type=jnp.float32
    )
    mixer_sum = (
        lax.psum_scatter(
            (product * piece_scale[:, None]).astype(jnp.bfloat16),
            "tp",
            scatter_dimension=0,
            tiled=True,
        )
        .astype(jnp.float32)
        .T
    )
    residual = (tokens.astype(jnp.float32) + mixer_sum).astype(jnp.bfloat16)
    full_up = lax.all_gather(weight_up.astype(jnp.bfloat16), "fs", axis=0, tiled=True)
    widened_mid = residual.astype(jnp.float32)
    squares_mid = lax.psum(jnp.sum(widened_mid * widened_mid, axis=1), "tp")
    inverse_mid = lax.rsqrt(squares_mid / feature_count + 1e-06)[:, None]
    gain_piece = norm2_gain
    normed_piece = (
        lax.all_gather(residual, "tp", axis=1, tiled=True).astype(jnp.float32)
        * inverse_mid
        * gain_piece
    ).astype(jnp.bfloat16)
    pre_up = jnp.dot(normed_piece, full_up, preferred_element_type=jnp.float32)
    hidden = jnp.square(jax.nn.relu(pre_up * scale_up)).astype(jnp.bfloat16)
    down_rounded = weight_down.astype(jnp.bfloat16)
    full_down = lax.all_gather(down_rounded, "fs", axis=1, tiled=True)
    columns = full_down
    piece_scale = down_scales
    product = lax.dot_general(
        columns, hidden, (((0,), (1,)), ((), ())), preferred_element_type=jnp.float32
    )
    channel_sum = (
        lax.psum_scatter(
            (product * piece_scale[:, None]).astype(jnp.bfloat16),
            "tp",
            scatter_dimension=0,
            tiled=True,
        )
        .astype(jnp.float32)
        .T
    )
    return (residual.astype(jnp.float32) + channel_sum).astype(jnp.bfloat16)


def solution(mesh):
    placed = (
        P(("grp", "fs"), "tp"),
        P(),
        P("fs", "tp"),
        P("fs", "tp"),
        P("tp"),
        P("tp"),
        P("tp"),
        P(),
        P(),
        P("tp", "fs"),
        P("fs"),
        P(),
        P("fs", "tp"),
        P("tp"),
        P("tp", "fs"),
        P("fs"),
    )
    return jax.shard_map(
        per_device, mesh=mesh, in_specs=placed, out_specs=P(("grp", "fs"), "tp"), check_vma=False
    )
```

profile of v0, /device:TPU:0, one launch (start us, length us, event | category | flops | bytes accessed | tf_op | source)
XLA Modules:
  0.0 601.0 jit_solution(15916655100287442903)
XLA Ops:
  6.5 0.0 copy-start
  6.5 0.0 all-gather.14.cloned.1.call-start
  6.5 1.8 convert_element_type.74
  8.3 0.0 all-gather.14.cloned.1.call-update
  8.3 0.0 all-gather.10.cloned.1.call-start
  8.4 0.7 all-gather.10.cloned.1.call-update
  9.1 0.0 all-gather.12.cloned.1.call-start
  9.1 1.8 convert_element_type.73
  10.9 0.0 all-gather.12.cloned.1.call-update
  10.9 0.0 all-gather.16.cloned.1.call-start
  11.0 1.8 convert_element_type.79
  12.7 0.0 all-gather.16.cloned.1.call-update
  12.8 0.0 reduce-scatter.3.cloned.1.call-start
  12.8 1.5 fusion.8
  14.3 8.4 %psum.28 = f32[1024]{0:T(1024)S(1)} all-reduce(f32[1024]{0:T(1024)S(1)} %fusion.8), channel_id=1, replica_groups=mesh['grp'=2,'fs'=4,'tp'=4] {'tp'}, use_global_device_ids=true, to_apply=%region_1.0 | all-reduce | flops 1024 | bytes 8192 | tf_op jit(solution)/shard_map/psum | solution.py:39
  22.7 12.7 %all-gather = f32[4,1,512]{2,1,0:T(1,128)S(1)} all-gather(f32[1,1,512]{2,1,0:T(1,128)} %bitcast.33), channel_id=1, replica_groups=mesh['grp'=2,'fs'=4,'tp'=4] {'fs'}, dimensions={0}, use_global_device_ids=true | all-gather | bytes 10240 | tf_op jit(solution)/shard_map/all_gather | solution.py:31
  35.4 0.0 copy-done
  35.4 0.0 copy-start.4
  35.4 0.0 copy-start.5
  35.4 0.0 copy-start.8
  35.5 4.3 all-gather.14.cloned.1.call-done
  39.8 35.4 %all-gather.10.cloned.1.call-done = bf16[1024,2048]{1,0:T(8,128)(2,1)} async-done(((bf16[1024,512]{1,0:T(8,128)(2,1)}), bf16[1024,2048]{1,0:T(8,128)(2,1)}) %all-gather.10.cloned.1.call-update) | async-done | bytes 4194320 | tf_op jit(solution)/shard_map/all_gather | solution.py:43
  75.2 4.2 fusion.45
  79.4 6.0 %all-reduce = (f32[1024]{0:T(1024)S(1)}, f32[1024]{0:T(1024)S(1)}) all-reduce(f32[1024]{0:T(1024)S(1)} %get-tuple-element.6, f32[1024]{0:T(1024)S(1)} %get-tuple-element.5), channel_id=1, replica_groups=mesh['grp'=2,'fs'=4,'tp'=4] {'tp'}, use_global_device_ids=true, to_apply=%region_5.0 | all-reduce | flops 2048 | bytes 16384 | tf_op jit(solution)/shard_map/psum | solution.py:52
  85.4 0.0 copy-done.4
  85.4 0.3 multiply_convert_fusion.21
  85.8 1.1 convolution_add_fusion
  86.9 17.9 %all-gather.12.cloned.1.call-done = bf16[2048,256]{1,0:T(8,128)(2,1)} async-done(((bf16[512,256]{1,0:T(8,128)(2,1)}), bf16[2048,256]{1,0:T(8,128)(2,1)}) %all-gather.12.cloned.1.call-update) | async-done | bytes 1048592 | tf_op jit(solution)/shard_map/all_gather | solution.py:35
  104.8 28.8 %all-gather.16.cloned.1.call-done = bf16[256,2048]{1,0:T(8,128)(2,1)} async-done(((bf16[256,512]{1,0:T(8,128)(2,1)}), bf16[256,2048]{1,0:T(8,128)(2,1)}) %all-gather.16.cloned.1.call-update) | async-done | bytes 1048592 | tf_op jit(solution)/shard_map/all_gather | solution.py:69
  133.6 0.0 copy-done.5
  133.6 0.0 copy-done.8
  133.6 9.3 %fusion.6 = bf16[2048,1024]{0,1:T(8,128)(2,1)} fusion(f32[2048]{0:T(1024)S(1)} %bitcast.31, bf16[256,2048]{1,0:T(8,128)(2,1)} %all-gather.16.cloned.1.call-done, f32[1024,256]{1,0:T(8,128)S(1)} %bitcast.30, bf16[2048,256]{1,0:T(8,128)(2,1)} %all-gather.12.cloned.1.call-done, bf16[1024,2048]{1,0:T(8,128)(2,1)} %all-gather.10.cloned.1.call-done, ...), kind=kOutput, calls=%fused_computation.9 | convolution fusion | flops 2162950144 | bytes 11555840 | tf_op jit(solution)/shard_map/dot_general | solution.py:72
  142.9 0.0 reduce-scatter.3.cloned.1.call-update
  142.9 0.0 copy-start.2
  142.9 0.0 all-gather.20.cloned.1.call-start
  143.0 3.9 convert_element_type.86
  146.9 0.0 copy-start.3
  146.9 0.0 copy-start.6
  146.9 0.0 copy-start.7
  146.9 0.0 all-gather.20.cloned.1.call-update
  146.9 0.0 all-gather.22.cloned.1.call-start
  147.0 4.4 convert_element_type.88
  151.4 0.0 all-gather.22.cloned.1.call-update
  151.4 0.0 all-gather.18.cloned.1.call-start
  151.5 35.4 %reduce-scatter.3.cloned.1.call-done = bf16[512,1024]{0,1:T(8,128)(2,1)} async-done(((bf16[2048,1024]{0,1:T(8,128)(2,1)}), bf16[512,1024]{0,1:T(8,128)(2,1)}) %reduce-scatter.3.cloned.1.call-update) | async-done | bytes 1048592 | tf_op jit(solution)/shard_map/reduce_scatter | solution.py:76
  186.8 0.0 copy-done.2
  186.8 2.6 fusion.10
  189.4 0.0 all-gather.18.cloned.1.call-update
  189.5 0.0 reduce-scatter.5.cloned.1.call-start
  189.5 0.0 copy-done.3
  189.5 12.0 %all-gather.1 = f32[4,1,512]{2,1,0:T(1,128)S(1)} all-gather(f32[1,1,512]{2,1,0:T(1,128)S(1)} %bitcast.34), channel_id=1, replica_groups=mesh['grp'=2,'fs'=4,'tp'=4] {'fs'}, dimensions={0}, use_global_device_ids=true | all-gather | bytes 10240 | tf_op jit(solution)/shard_map/all_gather | solution.py:32
  201.5 6.0 %psum.31 = f32[1024]{0:T(1024)S(1)} all-reduce(f32[1024]{0:T(1024)S(1)} %get-tuple-element.9), channel_id=1, replica_groups=mesh['grp'=2,'fs'=4,'tp'=4] {'tp'}, use_global_device_ids=true, to_apply=%region_8.9 | all-reduce | flops 1024 | bytes 8192 | tf_op jit(solution)/shard_map/psum | solution.py:88
  207.6 130.4 %all-gather.20.cloned.1.call-done = bf16[2048,2048]{1,0:T(8,128)(2,1)} async-done(((bf16[512,2048]{1,0:T(8,128)(2,1)}), bf16[2048,2048]{1,0:T(8,128)(2,1)}) %all-gather.20.cloned.1.call-update) | async-done | bytes 8388624 | tf_op jit(solution)/shard_map/all_gather | solution.py:86
  337.9 149.4 %all-gather.22.cloned.1.call-done = bf16[2048,2048]{1,0:T(8,128)(2,1)} async-done(((bf16[2048,512]{1,0:T(8,128)(2,1)}), bf16[2048,2048]{1,0:T(8,128)(2,1)}) %all-gather.22.cloned.1.call-update) | async-done | bytes 8388624 | tf_op jit(solution)/shard_map/all_gather | solution.py:99
  487.3 34.2 %all-gather.18.cloned.1.call-done = bf16[1024,2048]{1,0:T(8,128)(2,1)} async-done(((bf16[1024,512]{1,0:T(8,128)(2,1)}), bf16[1024,2048]{1,0:T(8,128)(2,1)}) %all-gather.18.cloned.1.call-update) | async-done | bytes 4194320 | tf_op jit(solution)/shard_map/all_gather | solution.py:92
  521.6 0.0 copy-done.6
  521.6 0.0 copy-done.7
  521.6 0.0 copy-start.1
  521.6 25.7 %fusion.7 = bf16[2048,1024]{0,1:T(8,128)(2,1)} fusion(f32[2048]{0:T(1024)S(1)} %bitcast.32, bf16[2048,2048]{1,0:T(8,128)(2,1)} %all-gather.22.cloned.1.call-done, bf16[2048,2048]{1,0:T(8,128)(2,1)} %all-gather.20.cloned.1.call-done, bf16[1024,2048]{1,0:T(8,128)(2,1)} %all-gather.18.cloned.1.call-done, f32[2048]{0:T(1024)S(1)} %copy-done.6, ...), kind=kOutput, calls=%fused_computation.10 | convolution fusion | flops 17200840704 | bytes 25194496 | tf_op jit(solution)/shard_map/dot_general | solution.py:102
  547.3 0.0 reduce-scatter.5.cloned.1.call-update
  547.3 44.6 %reduce-scatter.5.cloned.1.call-done = bf16[512,1024]{0,1:T(8,128)(2,1)} async-done(((bf16[2048,1024]{0,1:T(8,128)(2,1)}), bf16[512,1024]{0,1:T(8,128)(2,1)}) %reduce-scatter.5.cloned.1.call-update) | async-done | bytes 1048592 | tf_op jit(solution)/shard_map/reduce_scatter | solution.py:106
  591.9 0.0 copy-done.1
  591.9 2.5 fusion.11
  (4 shorter events, 0.0 us)
Async XLA Ops:
  6.5 28.9 %copy-start = (f32[4,128]{1,0:T(4,128)S(1)}, f32[4,128]{1,0:T(4,128)}, u32[]{:S(2)}) copy-start(f32[4,128]{1,0:T(4,128)} %param.24) | copy-start | bytes 6148
  6.5 33.2 %all-gather.14.cloned.1.call-start = ((), (), s32[]{:S(2)}) async-start(), calls=%async_computation.4 | async-start | bytes 1310720 | tf_op jit(solution)/shard_map/all_gather | solution.py:36
  8.3 66.9 %all-gather.10.cloned.1.call-start = ((), (), s32[]{:S(2)}) async-start(), calls=%async_computation.2 | async-start | bytes 5242880 | tf_op jit(solution)/shard_map/all_gather | solution.py:43
  9.1 95.7 %all-gather.12.cloned.1.call-start = ((), (), s32[]{:S(2)}) async-start(), calls=%async_computation.3 | async-start | bytes 1310720 | tf_op jit(solution)/shard_map/all_gather | solution.py:35
  10.9 122.7 %all-gather.16.cloned.1.call-start = ((), (), s32[]{:S(2)}) async-start(), calls=%async_computation.5 | async-start | bytes 1310720 | tf_op jit(solution)/shard_map/all_gather | solution.py:69
  12.8 174.1 %reduce-scatter.3.cloned.1.call-start = ((), (), s32[]{:S(2)}) async-start(), calls=%async_computation.6 | async-start | bytes 5242880 | tf_op jit(solution)/shard_map/reduce_scatter | solution.py:76
  35.4 50.0 %copy-start.4 = (f32[256]{0:T(256)S(1)}, f32[256]{0:T(256)}, u32[]{:S(2)}) copy-start(f32[256]{0:T(256)} %param.22) | copy-start | bytes 3076
  35.4 98.2 %copy-start.5 = (f32[2048]{0:T(1024)S(1)}, f32[2048]{0:T(1024)}, u32[]{:S(2)}) copy-start(f32[2048]{0:T(1024)} %param.17) | copy-start | bytes 24580
  35.4 98.2 %copy-start.8 = (f32[256]{0:T(256)S(1)}, f32[256]{0:T(256)}, u32[]{:S(2)}) copy-start(f32[256]{0:T(256)} %param.20) | copy-start | bytes 3076
  142.9 43.9 %copy-start.2 = (bf16[1024,512]{1,0:T(8,128)(2,1)S(1)}, bf16[1024,512]{1,0:T(8,128)(2,1)}, u32[]{:S(2)}) copy-start(bf16[1024,512]{1,0:T(8,128)(2,1)} %param.16) | copy-start | bytes 3145732
  142.9 195.0 %all-gather.20.cloned.1.call-start = ((), (), s32[]{:S(2)}) async-start(), calls=%async_computation.8 | async-start | bytes 10485760 | tf_op jit(solution)/shard_map/all_gather | solution.py:86
  146.9 42.6 %copy-start.3 = (f32[512]{0:T(512)S(1)}, f32[512]{0:T(512)}, u32[]{:S(2)}) copy-start(f32[512]{0:T(512)} %param.31) | copy-start | bytes 6148
  146.9 374.6 %copy-start.6 = (f32[2048]{0:T(1024)S(1)}, f32[2048]{0:T(1024)}, u32[]{:S(2)}) copy-start(f32[2048]{0:T(1024)} %param.29) | copy-start | bytes 24580
  146.9 374.6 %copy-start.7 = (f32[2048]{0:T(1024)S(1)}, f32[2048]{0:T(1024)}, u32[]{:S(2)}) copy-start(f32[2048]{0:T(1024)} %param.27) | copy-start | bytes 24580
  146.9 340.4 %all-gather.22.cloned.1.call-start = ((), (), s32[]{:S(2)}) async-start(), calls=%async_computation.9 | async-start | bytes 10485760 | tf_op jit(solution)/shard_map/all_gather | solution.py:99
  151.4 370.1 %all-gather.18.cloned.1.call-start = ((), (), s32[]{:S(2)}) async-start(), calls=%async_computation.7 | async-start | bytes 5242880 | tf_op jit(solution)/shard_map/all_gather | solution.py:92
  189.5 402.4 %reduce-scatter.5.cloned.1.call-start = ((), (), s32[]{:S(2)}) async-start(), calls=%async_computation.10 | async-start | bytes 5242880 | tf_op jit(solution)/shard_map/reduce_scatter | solution.py:106
  521.6 70.3 %copy-start.1 = (bf16[1024,512]{1,0:T(8,128)(2,1)S(1)}, bf16[1024,512]{1,0:T(8,128)(2,1)}, u32[]{:S(2)}) copy-start(bf16[1024,512]{1,0:T(8,128)(2,1)} %get-tuple-element.10) | copy-start | bytes 3145732
Sparse Core Ops, SparseCore 0:
  8.9 30.8 all-gather.13
  41.3 33.8 all-gather.9
  76.8 27.9 all-gather.11
  106.2 27.3 all-gather.15
  143.1 43.7 reduce-scatter.2
  188.3 149.6 all-gather.19
  339.5 147.7 all-gather.21
  488.9 32.6 all-gather.17
  547.5 44.3 reduce-scatter.4
where the time goes:
time: 601 us
  waiting for transfers between devices  481 us (80%)
  blocking collectives  45.1 us (8%)
  matrix products  40.3 us (7%)
  other arithmetic  20.6 us (3%)
  between operations  13.3 us (2%)
    all_gather x1, waiting for transfers between devices, per_device(): full_down = lax.all_gather(down_rounded, 'fs', axis=1, tiled=True)  149 us
    all_gather x1, waiting for transfers between devices, per_device(): lax.all_gather(weight_up.astype(jnp.bfloat16), 'fs', axis=0, tiled=True)  130 us
    reduce_scatter x2, waiting for transfers between devices, per_device(): lax.psum_scatter((product * piece_scale[:, None]).astype(jnp.bfloat16), '...  79.9 us
    all_gather x1, waiting for transfers between devices, per_device(): lax.all_gather(tokens, 'tp', axis=1, tiled=True).astype(jnp.float32)  35.4 us
    all_gather x1, waiting for transfers between devices, per_device(): lax.all_gather(residual, 'tp', axis=1, tiled=True).astype(jnp.float32)  34.2 us
    all_gather x1, waiting for transfers between devices, per_device(): full_out = lax.all_gather(out_rounded, 'fs', axis=1, tiled=True)  28.8 us
    dot_general x1, matrix products, per_device(): lax.dot_general(columns, hidden, (((0,), (1,)), ((), ())), preferred_elem...  25.7 us
    all_gather x1, waiting for transfers between devices, per_device(): lax.all_gather(weight_u.astype(jnp.bfloat16), 'fs', axis=0, tiled=True)  17.9 us
  transfers between devices with their start and end apart: 9, of which 9 were waited for; matrix products, arithmetic and copies ran while one was open for 4% of the time, Pallas kernels for 0%

commit v1 on v0

--- a/solution.py
+++ b/solution.py
@@ -96,7 +96,12 @@
     pre_up = jnp.dot(normed_piece, full_up, preferred_element_type=jnp.float32)
     hidden = jnp.square(jax.nn.relu(pre_up * scale_up)).astype(jnp.bfloat16)
     down_rounded = weight_down.astype(jnp.bfloat16)
-    full_down = lax.all_gather(down_rounded, "fs", axis=1, tiled=True)
+    ring = [down_rounded]
+    for hop in range(3):
+        ring.append(lax.ppermute(ring[-1], "fs", [(dev, (dev + 1) % 4) for dev in range(4)]))
+    full_down = jnp.roll(
+        jnp.concatenate(ring[::-1], axis=1), (lax.axis_index("fs") + 1) * ring[0].shape[1], axis=1
+    )
     columns = full_down
     piece_scale = down_scales
     product = lax.dot_general(

time: 601 us -> 540 us (0.90)
  waiting for transfers between devices: 481 us -> 278 us
  blocking collectives: 45.1 us -> 136 us
  starting transfers between devices: 0.33 us -> 36.3 us
  local copies, waits for them, and re-layouts: 0.05 us -> 14.6 us
    all_gather x1 -> x0, waiting for transfers between devices: 149 us -> none  [per_device(): full_down = lax.all_gather(down_rounded, 'fs', axis=1, tiled=True)]
    ppermute x0 -> x3, waiting for transfers between devices: none -> 138 us  [per_device(): lax.ppermute(ring[-1], 'fs', [(dev, (dev + 1) % 4) for dev in range(4)])]
    all_gather x1, waiting for transfers between devices: 130 us -> 0.01 us  [per_device(): lax.all_gather(weight_up.astype(jnp.bfloat16), 'fs', axis=0, tiled=True)]
    all_gather x1, blocking collectives: 12 us -> 104 us  [per_device(): lax.all_gather(scale_down, 'fs', axis=0, tiled=True)]
    ppermute x0 -> x3, starting transfers between devices: none -> 36 us  [per_device(): lax.ppermute(ring[-1], 'fs', [(dev, (dev + 1) % 4) for dev in range(4)])]
    reduce_scatter x2, waiting for transfers between devices: 79.9 us -> 44.6 us  [per_device(): lax.psum_scatter((product * piece_scale[:, None]).astype(jnp.bfloat16), '...]
    all_gather x1, waiting for transfers between devices: 34.2 us -> 7.22 us  [per_device(): lax.all_gather(residual, 'tp', axis=1, tiled=True).astype(jnp.float32)]
    unnamed x18 -> x30, local copies, waits for them, and re-layouts: 0.04 us -> 14.6 us
  transfers between devices with their start and end apart: 9 -> 11, of which waited for: 9 -> 8; matrix products, arithmetic and copies ran while one was open for 4% -> 6% of each run, Pallas kernels for 0% -> 0%
where the time goes in v1:
time: 540 us
  waiting for transfers between devices  278 us (51%)
  blocking collectives  136 us (25%)
  matrix products  40.4 us (7%)
  starting transfers between devices  36.3 us (7%)
  other arithmetic  20.1 us (4%)
  local copies, waits for them, and re-layouts  14.6 us (3%)
  between operations  13.7 us (3%)
    ppermute x3, waiting for transfers between devices, per_device(): lax.ppermute(ring[-1], 'fs', [(dev, (dev + 1) % 4) for dev in range(4)])  138 us
    all_gather x1, blocking collectives, per_device(): lax.all_gather(scale_down, 'fs', axis=0, tiled=True)  104 us
    reduce_scatter x2, waiting for transfers between devices, per_device(): lax.psum_scatter((product * piece_scale[:, None]).astype(jnp.bfloat16), '...  44.6 us
    ppermute x3, starting transfers between devices, per_device(): lax.ppermute(ring[-1], 'fs', [(dev, (dev + 1) % 4) for dev in range(4)])  36 us
    all_gather x1, waiting for transfers between devices, per_device(): lax.all_gather(tokens, 'tp', axis=1, tiled=True).astype(jnp.float32)  35.4 us
    all_gather x1, waiting for transfers between devices, per_device(): lax.all_gather(weight_u.astype(jnp.bfloat16), 'fs', axis=0, tiled=True)  28.8 us
    dot_general x1, matrix products, per_device(): lax.dot_general(columns, hidden, (((0,), (1,)), ((), ())), preferred_elem...  25.7 us
    all_gather x1, waiting for transfers between devices, per_device(): full_out = lax.all_gather(out_rounded, 'fs', axis=1, tiled=True)  17.9 us
  transfers between devices with their start and end apart: 11, of which 8 were waited for; matrix products, arithmetic and copies ran while one was open for 6% of the time, Pallas kernels for 0%

profile of v1, /device:TPU:0, one launch (start us, length us, event | category | flops | bytes accessed | tf_op | source)
XLA Modules:
  0.0 539.6 jit_solution(9207090641243520211)
XLA Ops:
  6.5 0.0 all-gather.13.cloned.1.call-start
  6.5 1.8 convert_element_type.71
  8.3 0.0 all-gather.13.cloned.1.call-update
  8.4 0.0 all-gather.9.cloned.1.call-start
  8.4 0.7 all-gather.9.cloned.1.call-update
  9.1 0.0 all-gather.15.cloned.1.call-start
  9.2 1.8 convert_element_type.76
  10.9 0.0 all-gather.15.cloned.1.call-update
  11.0 0.0 all-gather.11.cloned.1.call-start
  11.0 1.8 convert_element_type.70
  12.8 0.0 all-gather.11.cloned.1.call-update
  12.8 0.0 reduce-scatter.3.cloned.1.call-start
  12.9 1.5 fusion.8
  14.4 14.0 %all-gather = f32[4,1,512]{2,1,0:T(1,128)S(1)} all-gather(f32[1,1,512]{2,1,0:T(1,128)} %bitcast.30), channel_id=1, replica_groups=mesh['grp'=2,'fs'=4,'tp'=4] {'fs'}, dimensions={0}, use_global_device_ids=true | all-gather | bytes 10240 | tf_op jit(solution)/shard_map/all_gather | solution.py:31
  28.4 6.0 %psum.28 = f32[1024]{0:T(1024)S(1)} all-reduce(f32[1024]{0:T(1024)S(1)} %fusion.8), channel_id=1, replica_groups=mesh['grp'=2,'fs'=4,'tp'=4] {'tp'}, use_global_device_ids=true, to_apply=%region_1.0 | all-reduce | flops 1024 | bytes 8192 | tf_op jit(solution)/shard_map/psum | solution.py:39
  34.4 0.0 copy-done
  34.5 0.0 copy-start.7
  34.5 0.0 copy-start.8
  34.5 0.0 copy-start.11
  34.5 5.2 all-gather.13.cloned.1.call-done
  39.7 35.4 %all-gather.9.cloned.1.call-done = bf16[1024,2048]{1,0:T(8,128)(2,1)} async-done(((bf16[1024,512]{1,0:T(8,128)(2,1)}), bf16[1024,2048]{1,0:T(8,128)(2,1)}) %all-gather.9.cloned.1.call-update) | async-done | bytes 4194320 | tf_op jit(solution)/shard_map/all_gather | solution.py:43
  75.2 4.2 fusion.47
  79.3 6.0 %all-reduce = (f32[1024]{0:T(1024)S(1)}, f32[1024]{0:T(1024)S(1)}) all-reduce(f32[1024]{0:T(1024)S(1)} %get-tuple-element.6, f32[1024]{0:T(1024)S(1)} %get-tuple-element.5), channel_id=1, replica_groups=mesh['grp'=2,'fs'=4,'tp'=4] {'tp'}, use_global_device_ids=true, to_apply=%region_5.0 | all-reduce | flops 2048 | bytes 16384 | tf_op jit(solution)/shard_map/psum | solution.py:52
  85.4 0.3 multiply_convert_fusion.22
  85.7 1.1 convolution_add_fusion
  86.9 17.9 %all-gather.15.cloned.1.call-done = bf16[256,2048]{1,0:T(8,128)(2,1)} async-done(((bf16[256,512]{1,0:T(8,128)(2,1)}), bf16[256,2048]{1,0:T(8,128)(2,1)}) %all-gather.15.cloned.1.call-update) | async-done | bytes 1048592 | tf_op jit(solution)/shard_map/all_gather | solution.py:69
  104.7 28.8 %all-gather.11.cloned.1.call-done = bf16[2048,256]{1,0:T(8,128)(2,1)} async-done(((bf16[512,256]{1,0:T(8,128)(2,1)}), bf16[2048,256]{1,0:T(8,128)(2,1)}) %all-gather.11.cloned.1.call-update) | async-done | bytes 1048592 | tf_op jit(solution)/shard_map/all_gather | solution.py:35
  133.6 9.3 %fusion.7 = bf16[2048,1024]{0,1:T(8,128)(2,1)} fusion(f32[2048]{0:T(1024)S(1)} %bitcast.28, bf16[256,2048]{1,0:T(8,128)(2,1)} %all-gather.15.cloned.1.call-done, f32[1024,256]{1,0:T(8,128)S(1)} %bitcast.27, bf16[2048,256]{1,0:T(8,128)(2,1)} %all-gather.11.cloned.1.call-done, bf16[1024,2048]{1,0:T(8,128)(2,1)} %all-gather.9.cloned.1.call-done, ...), kind=kOutput, calls=%fused_computation.9 | convolution fusion | flops 2162950144 | bytes 11555840 | tf_op jit(solution)/shard_map/dot_general | solution.py:72
  142.9 0.0 reduce-scatter.3.cloned.1.call-update
  142.9 0.0 copy-start.4
  142.9 0.0 copy-start.6
  143.0 0.0 all-gather.19.cloned.1.call-start
  143.0 3.9 convert_element_type.84
  146.9 0.0 all-gather.19.cloned.1.call-update
  147.0 0.0 all-gather.17.cloned.1.call-start
  147.0 3.0 convert_element_type.81
  150.1 1.6 collective-permute-start
  151.7 47.0 %collective-permute-done = bf16[2048,512]{1,0:T(8,128)(2,1)S(1)} collective-permute-done((bf16[2048,512]{1,0:T(8,128)(2,1)S(1)}, bf16[2048,512]{1,0:T(8,128)(2,1)S(1)}, u32[]{:S(2)}, u32[]{:S(2)}) %collective-permute-start) | collective-permute-done | bytes 2097184 | tf_op jit(solution)/shard_map/ppermute | solution.py:101
  198.7 0.0 collective-permute-start.1
  198.7 2.7 fusion.10
  201.4 0.0 all-gather.17.cloned.1.call-update
  201.4 0.0 reduce-scatter.5.cloned.1.call-start
  201.4 91.2 %collective-permute-done.1 = bf16[2048,512]{1,0:T(8,128)(2,1)} collective-permute-done((bf16[2048,512]{1,0:T(8,128)(2,1)S(1)}, bf16[2048,512]{1,0:T(8,128)(2,1)}, u32[]{:S(2)}, u32[]{:S(2)}) %collective-permute-start.1) | collective-permute-done | bytes 2097184 | tf_op jit(solution)/shard_map/ppermute | solution.py:101
  292.6 34.4 %collective-permute-start.2 = (bf16[2048,512]{1,0:T(8,128)(2,1)}, bf16[2048,512]{1,0:T(8,128)(2,1)}, u32[]{:S(2)}, u32[]{:S(2)}) collective-permute-start(bf16[2048,512]{1,0:T(8,128)(2,1)} %collective-permute-done.1), channel_id=1, source_target_pairs={{0,4},{4,8},{8,12},{12,0},{1,5},{5,9},{9,13},{13,1},{2,6},{6,10},{... | collective-permute-start | bytes 6291464 | tf_op jit(solution)/shard_map/ppermute | solution.py:101
  327.0 103.9 %all-gather.1 = f32[4,1,512]{2,1,0:T(1,128)S(1)} all-gather(f32[1,1,512]{2,1,0:T(1,128)S(1)} %bitcast.31), channel_id=1, replica_groups=mesh['grp'=2,'fs'=4,'tp'=4] {'fs'}, dimensions={0}, use_global_device_ids=true | all-gather | bytes 10240 | tf_op jit(solution)/shard_map/all_gather | solution.py:32
  430.9 0.0 collective-permute-done.2
  430.9 2.1 constant_dynamic-update-slice_fusion.7
  433.1 2.2 constant_dynamic-update-slice_fusion.6
  435.2 0.3 constant_dynamic-update-slice_fusion.5
  435.6 0.3 constant_dynamic-update-slice_fusion.4
  435.9 1.9 constant_dynamic-update-slice_fusion.3
  437.8 0.0 copy-start.9
  437.9 0.0 copy-start.10
  437.9 1.9 constant_dynamic-update-slice_fusion.2
  439.8 0.3 constant_dynamic-update-slice_fusion.1
  440.1 0.3 constant_dynamic-update-slice_fusion
  440.5 5.7 %copy-done.5 = bf16[2048,4096]{1,0:T(8,128)(2,1)} copy-done((bf16[2048,4096]{1,0:T(8,128)(2,1)}, bf16[2048,4096]{1,0:T(8,128)(2,1)S(1)}, u32[]{:S(2)}) %copy-start.5) | copy-done | bytes 16777240
  446.2 6.5 %psum.31 = f32[1024]{0:T(1024)S(1)} all-reduce(f32[1024]{0:T(1024)S(1)} %get-tuple-element.9), channel_id=1, replica_groups=mesh['grp'=2,'fs'=4,'tp'=4] {'tp'}, use_global_device_ids=true, to_apply=%region_8.9 | all-reduce | flops 1024 | bytes 8192 | tf_op jit(solution)/shard_map/psum | solution.py:88
  452.7 0.0 all-gather.19.cloned.1.call-done
  452.7 7.2 %all-gather.17.cloned.1.call-done = bf16[1024,2048]{1,0:T(8,128)(2,1)} async-done(((bf16[1024,512]{1,0:T(8,128)(2,1)}), bf16[1024,2048]{1,0:T(8,128)(2,1)}) %all-gather.17.cloned.1.call-update) | async-done | bytes 4194320 | tf_op jit(solution)/shard_map/all_gather | solution.py:92
  459.9 25.7 %multiply_convert_fusion = bf16[2048,1024]{0,1:T(8,128)(2,1)} fusion(f32[2048]{0:T(1024)S(1)} %bitcast.29, bf16[2048,4096]{1,0:T(8,128)(2,1)} %copy-done.5, s32[]{:T(128)S(6)} %select_n.38, bf16[2048,2048]{1,0:T(8,128)(2,1)} %all-gather.19.cloned.1.call-done, bf16[1024,2048]{1,0:T(8,128)(2,1)} %all-gather.17.cloned.1.call-done, f32[2048]{0:T(1024)S(1)} %copy-done.9, ...), kind=kOutput, calls=%fused_computation | convolution fusion | flops 17200840704 | bytes 25194500 | tf_op jit(solution)/shard_map/dot_general | solution.py:107
  485.7 0.0 reduce-scatter.5.cloned.1.call-update
  485.7 44.6 %reduce-scatter.5.cloned.1.call-done = bf16[512,1024]{0,1:T(8,128)(2,1)} async-done(((bf16[2048,1024]{0,1:T(8,128)(2,1)}), bf16[512,1024]{0,1:T(8,128)(2,1)}) %reduce-scatter.5.cloned.1.call-update) | async-done | bytes 1048592 | tf_op jit(solution)/shard_map/reduce_scatter | solution.py:111
  530.3 2.5 fusion.11
  (20 shorter events, 0.1 us)
Async XLA Ops:
  6.5 27.9 %copy-start = (f32[4,128]{1,0:T(4,128)S(1)}, f32[4,128]{1,0:T(4,128)}, u32[]{:S(2)}) copy-start(f32[4,128]{1,0:T(4,128)} %param.24) | copy-start | bytes 6148
  6.5 33.2 %all-gather.13.cloned.1.call-start = ((), (), s32[]{:S(2)}) async-start(), calls=%async_computation.4 | async-start | bytes 1310720 | tf_op jit(solution)/shard_map/all_gather | solution.py:36
  8.4 66.8 %all-gather.9.cloned.1.call-start = ((), (), s32[]{:S(2)}) async-start(), calls=%async_computation.2 | async-start | bytes 5242880 | tf_op jit(solution)/shard_map/all_gather | solution.py:43
  9.1 95.6 %all-gather.15.cloned.1.call-start = ((), (), s32[]{:S(2)}) async-start(), calls=%async_computation.5 | async-start | bytes 1310720 | tf_op jit(solution)/shard_map/all_gather | solution.py:69
  11.0 122.6 %all-gather.11.cloned.1.call-start = ((), (), s32[]{:S(2)}) async-start(), calls=%async_computation.3 | async-start | bytes 1310720 | tf_op jit(solution)/shard_map/all_gather | solution.py:35
  12.8 185.9 %reduce-scatter.3.cloned.1.call-start = ((), (), s32[]{:S(2)}) async-start(), calls=%async_computation.6 | async-start | bytes 5242880 | tf_op jit(solution)/shard_map/reduce_scatter | solution.py:76
  34.5 50.9 %copy-start.7 = (f32[256]{0:T(256)S(1)}, f32[256]{0:T(256)}, u32[]{:S(2)}) copy-start(f32[256]{0:T(256)} %param.22) | copy-start | bytes 3076
  34.5 99.1 %copy-start.8 = (f32[2048]{0:T(1024)S(1)}, f32[2048]{0:T(1024)}, u32[]{:S(2)}) copy-start(f32[2048]{0:T(1024)} %param.17) | copy-start | bytes 24580
  34.5 99.1 %copy-start.11 = (f32[256]{0:T(256)S(1)}, f32[256]{0:T(256)}, u32[]{:S(2)}) copy-start(f32[256]{0:T(256)} %param.20) | copy-start | bytes 3076
  142.9 55.8 %copy-start.4 = (bf16[1024,512]{1,0:T(8,128)(2,1)S(1)}, bf16[1024,512]{1,0:T(8,128)(2,1)}, u32[]{:S(2)}) copy-start(bf16[1024,512]{1,0:T(8,128)(2,1)} %param.16) | copy-start | bytes 3145732
  142.9 184.1 %copy-start.6 = (f32[512]{0:T(512)S(1)}, f32[512]{0:T(512)}, u32[]{:S(2)}) copy-start(f32[512]{0:T(512)} %param.31) | copy-start | bytes 6148
  143.0 309.7 %all-gather.19.cloned.1.call-start = ((), (), s32[]{:S(2)}) async-start(), calls=%async_computation.8 | async-start | bytes 10485760 | tf_op jit(solution)/shard_map/all_gather | solution.py:86
  147.0 313.0 %all-gather.17.cloned.1.call-start = ((), (), s32[]{:S(2)}) async-start(), calls=%async_computation.7 | async-start | bytes 5242880 | tf_op jit(solution)/shard_map/all_gather | solution.py:92
  150.1 48.6 %collective-permute-start = (bf16[2048,512]{1,0:T(8,128)(2,1)S(1)}, bf16[2048,512]{1,0:T(8,128)(2,1)S(1)}, u32[]{:S(2)}, u32[]{:S(2)}) collective-permute-start(bf16[2048,512]{1,0:T(8,128)(2,1)S(1)} %convert_element_type.81), channel_id=1, source_target_pairs={{0,4},{4,8},{8,12},{12,0},{1,5},{5,9},{9,13},{13,1},{2,6},{6,10},{... | collective-permute-start | bytes 6291464 | tf_op jit(solution)/shard_map/ppermute | solution.py:101
  198.7 93.9 %collective-permute-start.1 = (bf16[2048,512]{1,0:T(8,128)(2,1)S(1)}, bf16[2048,512]{1,0:T(8,128)(2,1)}, u32[]{:S(2)}, u32[]{:S(2)}) collective-permute-start(bf16[2048,512]{1,0:T(8,128)(2,1)S(1)} %collective-permute-done), channel_id=1, source_target_pairs={{0,4},{4,8},{8,12},{12,0},{1,5},{5,9},{9,13},{13,1},{2,6},{6,10},{... | collective-permute-start | bytes 6291464 | tf_op jit(solution)/shard_map/ppermute | solution.py:101
  201.4 328.9 %reduce-scatter.5.cloned.1.call-start = ((), (), s32[]{:S(2)}) async-start(), calls=%async_computation.9 | async-start | bytes 5242880 | tf_op jit(solution)/shard_map/reduce_scatter | solution.py:111
  292.6 138.3 %collective-permute-start.2 = (bf16[2048,512]{1,0:T(8,128)(2,1)}, bf16[2048,512]{1,0:T(8,128)(2,1)}, u32[]{:S(2)}, u32[]{:S(2)}) collective-permute-start(bf16[2048,512]{1,0:T(8,128)(2,1)} %collective-permute-done.1), channel_id=1, source_target_pairs={{0,4},{4,8},{8,12},{12,0},{1,5},{5,9},{9,13},{13,1},{2,6},{6,10},{... | collective-permute-start | bytes 6291464 | tf_op jit(solution)/shard_map/ppermute | solution.py:101
  327.0 108.6 %copy-start.2 = (f32[2048,512]{1,0:T(8,128)S(1)}, f32[2048,512]{1,0:T(8,128)}, u32[]{:S(2)}) copy-start(f32[2048,512]{1,0:T(8,128)} %param.30) | copy-start | bytes 12582916
  437.8 22.1 %copy-start.9 = (f32[2048]{0:T(1024)S(1)}, f32[2048]{0:T(1024)}, u32[]{:S(2)}) copy-start(f32[2048]{0:T(1024)} %param.29) | copy-start | bytes 24580
  437.9 22.1 %copy-start.10 = (f32[2048]{0:T(1024)S(1)}, f32[2048]{0:T(1024)}, u32[]{:S(2)}) copy-start(f32[2048]{0:T(1024)} %param.27) | copy-start | bytes 24580
  440.5 5.7 %copy-start.5 = (bf16[2048,4096]{1,0:T(8,128)(2,1)}, bf16[2048,4096]{1,0:T(8,128)(2,1)S(1)}, u32[]{:S(2)}) copy-start(bf16[2048,4096]{1,0:T(8,128)(2,1)S(1)} %constant_dynamic-update-slice_fusion) | copy-start | bytes 50331652
  459.9 70.3 %copy-start.3 = (bf16[1024,512]{1,0:T(8,128)(2,1)S(1)}, bf16[1024,512]{1,0:T(8,128)(2,1)}, u32[]{:S(2)}) copy-start(bf16[1024,512]{1,0:T(8,128)(2,1)} %get-tuple-element.10) | copy-start | bytes 3145732
  459.9 72.9 %copy-start.1 = (f32[4,128]{1,0:T(4,128)S(1)}, f32[4,128]{1,0:T(4,128)}, u32[]{:S(2)}) copy-start(f32[4,128]{1,0:T(4,128)} %param.24) | copy-start | bytes 6148
Sparse Core Ops, SparseCore 0:
  8.9 30.7 all-gather.12
  41.3 33.8 all-gather.8
  76.7 27.9 all-gather.14
  106.2 27.3 all-gather.10
  143.0 43.7 reduce-scatter.2
  188.3 238.4 all-gather.18
  428.3 31.5 all-gather.16
  485.8 44.3 reduce-scatter.4
